TPU v7x, 32 devices: a whole 2x2x4 slice. The times are simulated.
32 devices in a mesh: ep: 16 (over z, x, core), tp: 2 (over y).
Axes of the slice: x: 2, y: 2, z: 4, core: 2. Of those that a mesh axis runs over, the one named last changes fastest.
Arguments:
- tokens: bfloat16 [256, 1024], P('ep'), may hold values from -6 to 6
- old_state: float32 [256, 4, 128, 128], P('ep', 'tp'), may hold values from -6 to 6
- query_weight: bfloat16 [1024, 512], P(None, 'tp'), may hold values from -0.1875 to 0.1875
- forget_weight: bfloat16 [1024, 512], P(None, 'tp'), may hold values from -0.1875 to 0.1875
- input_weight: bfloat16 [1024, 512], P(None, 'tp'), may hold values from -0.1875 to 0.1875
- lower_bound: float32 [512], P('tp'), may hold values from 0 to 0.9
- head_gain: float32 [4, 128], P('tp'), may hold values from 0.1 to 1.9
- out_weight: bfloat16 [512, 1024], P('tp'), may hold values from -0.25 to 0.25
- mix_gain: float32 [1024], replicated, may hold values from 0.1 to 1.9
- ffn_gain: float32 [1024], replicated, may hold values from 0.1 to 1.9
- group_weight: bfloat16 [1024, 4], replicated, may hold values from -0.1875 to 0.1875
- expert_weight: bfloat16 [1024, 16], replicated, may hold values from -0.1875 to 0.1875
- routes: int32 [256, 6], P('ep'), may hold values from 0 to 15, all different within a row; in each aligned block of 16 rows (0 to 15, 16 to 31, ...) at most 12 rows name the same one
- gate_weight: bfloat16 [16, 1024, 1024], P('ep', None, 'tp'), may hold values from -0.1875 to 0.1875
- up_weight: bfloat16 [16, 1024, 1024], P('ep', None, 'tp'), may hold values from -0.1875 to 0.1875
- down_weight: bfloat16 [16, 1024, 1024], P('ep', None, 'tp'), may hold values from -0.1875 to 0.1875
Outputs:
- layer_out: bfloat16 [256, 1024], P('ep', 'tp')
- new_state: float32 [256, 4, 128, 128], P('ep', 'tp')
Inputs may be any that keep to these rules, and one draw needn't show every extreme that they name: `routes`: each row names 6 different experts. In each aligned block of 16 rows (the rows of one device) no expert is named more than 12 times, a bound that some block reaches.
All inputs are finite; a program needn't handle non-finite values.
Results may differ from a plain program's by a relative error of at most 0.011.
Values may be sent and summed in bfloat16 or wider, within the bound.
A program may use at most 64 MiB of HBM per device.

v0:
```python
import jax
import jax.numpy as jnp
from jax import lax
from jax.sharding import PartitionSpec as P

epsilon = 1e-06


def scaled_rms(values, gain):
    return values * lax.rsqrt(jnp.mean(values * values, axis=-1, keepdims=True) + epsilon) * gain


def local(
    tokens,
    old_state,
    query_weight,
    forget_weight,
    input_weight,
    lower_bound,
    head_gain,
    out_weight,
    mix_gain,
    ffn_gain,
    group_weight,
    expert_weight,
    routes,
    gate_weight,
    up_weight,
    down_weight,
):
    seq_count, model_width = tokens.shape
    heads_local, head_size = (old_state.shape[1], old_state.shape[2])
    tp_size = lax.axis_size("tp")
    tp_rank = lax.axis_index("tp")
    part_width = model_width // tp_size
    resident = tokens.astype(jnp.float32)
    normed = scaled_rms(resident, mix_gain).astype(jnp.bfloat16)
    query_pre = jnp.dot(normed, query_weight, preferred_element_type=jnp.float32)
    forget_pre = jnp.dot(normed, forget_weight, preferred_element_type=jnp.float32)
    input_pre = jnp.dot(normed, input_weight, preferred_element_type=jnp.float32)
    query = jax.nn.silu(query_pre).reshape(seq_count, heads_local, head_size)
    forget = (lower_bound + (1.0 - lower_bound) * jax.nn.sigmoid(forget_pre)).reshape(
        seq_count, heads_local, head_size
    )
    value = input_pre.reshape(seq_count, heads_local, head_size)
    new_state = forget[..., None] * old_state + (1.0 - forget)[..., None] * value[:, :, None, :]
    readout = jnp.sum(new_state * query[..., None], axis=2)
    head_out = (
        scaled_rms(readout, head_gain)
        .astype(jnp.bfloat16)
        .reshape(seq_count, heads_local * head_size)
    )
    head_part = jnp.dot(head_out, out_weight, preferred_element_type=jnp.float32)
    mixed = lax.psum(head_part.astype(jnp.bfloat16), "tp")
    residual = (resident + mixed.astype(jnp.float32)).astype(jnp.bfloat16)
    ffn_in = scaled_rms(residual.astype(jnp.float32), ffn_gain).astype(jnp.bfloat16)
    experts = expert_weight.shape[1]
    groups = group_weight.shape[1]
    top_count = routes.shape[1]
    group_raw = jnp.exp(jnp.dot(ffn_in, group_weight, preferred_element_type=jnp.float32))
    group_prob = group_raw / jnp.sum(group_raw, axis=-1, keepdims=True)
    expert_raw = jnp.exp(
        jnp.dot(ffn_in, expert_weight, preferred_element_type=jnp.float32)
    ).reshape(seq_count, groups, experts // groups)
    expert_prob = (
        expert_raw / jnp.sum(expert_raw, axis=-1, keepdims=True) * group_prob[:, :, None]
    ).reshape(seq_count, experts)
    expert_ids = jnp.arange(experts, dtype=jnp.int32)
    chosen = routes[:, :, None] == expert_ids[None, None, :]
    weight = jnp.sum(jnp.where(chosen, expert_prob[:, None, :], 0.0), axis=-1)
    gate = weight / jnp.sum(weight, axis=-1, keepdims=True)
    capacity = min(seq_count, max(2, 2 * seq_count * top_count // experts))
    flat = routes.reshape(-1)
    hits = (flat[:, None] == expert_ids[None, :]).astype(jnp.int32)
    before = jnp.cumsum(hits, axis=0) - hits
    slots = jnp.sum(hits * before, axis=1)
    target = flat * capacity + slots
    slot_ids = jnp.arange(experts * capacity, dtype=jnp.int32)
    spread = jnp.sum(
        (slot_ids[:, None, None] == target.reshape(seq_count, top_count)[None, :, :]).astype(
            jnp.int32
        ),
        axis=2,
    ).astype(jnp.bfloat16)
    choose = (target[:, None] == slot_ids[None, :]).astype(jnp.bfloat16)
    outgoing = (
        jnp.dot(spread, ffn_in, preferred_element_type=jnp.float32)
        .astype(jnp.bfloat16)
        .reshape(experts, capacity, model_width)
    )
    arrived = lax.all_to_all(outgoing, "ep", split_axis=0, concat_axis=1, tiled=True)
    gate_hidden = jnp.einsum(
        "erd,edf->erf", arrived, gate_weight, preferred_element_type=jnp.float32
    )
    up_hidden = jnp.einsum("erd,edf->erf", arrived, up_weight, preferred_element_type=jnp.float32)
    hidden = (jax.nn.silu(gate_hidden) * up_hidden).astype(jnp.bfloat16)
    produced = jnp.einsum(
        "erf,efd->erd",
        lax.all_gather(hidden, "tp", axis=2, tiled=True),
        down_weight,
        preferred_element_type=jnp.float32,
    ).astype(jnp.bfloat16)
    returned = lax.all_to_all(produced, "ep", split_axis=1, concat_axis=0, tiled=True)
    picked = jnp.dot(
        choose, returned.reshape(experts * capacity, part_width), preferred_element_type=jnp.float32
    ).reshape(seq_count, top_count, part_width)
    mixture = jnp.sum(gate[:, :, None] * picked, axis=1)
    own_resid = lax.dynamic_slice_in_dim(residual, tp_rank * part_width, part_width, 1).astype(
        jnp.float32
    )
    layer_out = (own_resid + mixture).astype(jnp.bfloat16)
    return (layer_out, new_state)


def solution(mesh):
    in_specs = (
        P("ep", None),
        P("ep", "tp", None, None),
        P(None, "tp"),
        P(None, "tp"),
        P(None, "tp"),
        P("tp"),
        P("tp", None),
        P("tp", None),
        P(),
        P(),
        P(),
        P(),
        P("ep", None),
        P("ep", None, "tp"),
        P("ep", None, "tp"),
        P("ep", None, "tp"),
    )
    out_specs = (P("ep", "tp"), P("ep", "tp", None, None))
    return jax.shard_map(local, mesh=mesh, in_specs=in_specs, out_specs=out_specs, check_vma=False)
```

profile of v0, /device:TPU:0, one launch (start us, length us, event | category | flops | bytes accessed | tf_op | source)
XLA Modules:
  0.0 71.4 jit_solution(7429910828382578727)
XLA Ops:
  0.6 0.0 copy-start
  0.6 0.0 copy-start.1
  0.7 0.9 %copy.77 = s32[16,6]{1,0:T(8,128)S(1)} copy(s32[16,6]{0,1:T(8,128)} %param.28) | data formatting | bytes 768 | tf_op args[12]
  1.6 0.1 eq.73
  1.7 0.1 fusion.25
  1.8 0.1 reduce_window_sum.11
  1.9 0.2 select_reduce_fusion.2
  2.1 0.1 reduce_sum.110
  2.1 0.1 copy.78
  2.2 0.7 multiply_add_fusion.1
  2.9 0.1 convert_reduce_fusion
  3.0 0.9 %fusion.20 = f32[16]{0:T(128)S(1)} fusion(bf16[16,1024]{1,0:T(8,128)(2,1)} %param.16), kind=kLoop, calls=%fused_computation.37 | loop fusion | flops 49136 | bytes 32832 | tf_op jit(solution)/shard_map/reduce_sum | solution.py:10
  3.9 1.3 %divide_multiply_fusion = f32[16,256]{1,0:T(8,128)S(1)} fusion(bf16[1024,256]{1,0:T(8,128)(2,1)} %param.18, bf16[16,1024]{1,0:T(8,128)(2,1)} %param.16, f32[1024]{0:T(1024)} %param.24, f32[16]{0:T(128)S(1)} %add_rsqrt_fusion.2), kind=kOutput, calls=%fused_computation.53 | convolution fusion | flops 8470528 | bytes 577600 | tf_op jit(solution)/shard_map/dot_general | solution.py:38
  5.3 1.3 %fusion.33 = f32[16,256]{1,0:T(8,128)S(1)} fusion(bf16[1024,256]{1,0:T(8,128)(2,1)} %param.20, bf16[16,1024]{1,0:T(8,128)(2,1)} %param.16, f32[1024]{0:T(1024)} %param.24, f32[16]{0:T(128)S(1)} %add_rsqrt_fusion.2), kind=kOutput, calls=%fused_computation.67 | convolution fusion | flops 8454144 | bytes 577600 | tf_op jit(solution)/shard_map/dot_general | solution.py:40
  6.6 0.7 broadcast_subtract_fusion.1
  7.3 1.3 %fusion.8 = f32[16,256]{1,0:T(8,128)S(1)} fusion(bf16[1024,256]{1,0:T(8,128)(2,1)} %param.19, f32[256]{0:T(256)S(1)} %broadcast_subtract_fusion.1, f32[256]{0:T(256)} %param.21, bf16[16,1024]{1,0:T(8,128)(2,1)} %param.16, f32[1024]{0:T(1024)} %param.24, f32[16]{0:T(128)S(1)} %add_rsqrt_fusion.2), kind=kOutput, calls=%fused_computation.16 | convolution fusion | flops 8474624 | bytes 579648 | tf_op jit(solution)/shard_map/dot_general | solution.py:39
  8.6 0.0 copy-done.1
  8.6 0.0 copy-start.6
  8.6 0.0 copy-start.3
  8.7 0.0 copy-start.5
  8.7 3.0 %multiply_reduce_fusion = (f32[16,2,128]{2,1,0:T(2,128)S(1)}, f32[16,2,128,128]{3,2,1,0:T(8,128)}) fusion(f32[16,2,128]{2,1,0:T(2,128)S(1)} %mul.173, f32[16,2,128]{2,1,0:T(2,128)S(1)} %mul.169, f32[16,2,128]{2,1,0:T(2,128)S(1)} %broadcast_subtract_fusion, f32[16,2,128,128]{3,2,1,0:T(8,128)S(1)} %copy-done.1, f32[16,2,128]{2,1,0:T(2,128)S(1)} %mul.165), kind=kLoop, calls=%fused_computation.1 | loop fusion | flops 2617344 | bytes 4276224 | tf_op jit(solution)/shard_map/reduce_sum | solution.py:47
  11.7 0.0 copy-start.9
  11.7 0.0 copy-start.8
  11.7 0.1 fusion.27
  11.8 0.1 copy.73
  11.9 0.1 broadcast_multiply_fusion
  12.0 0.0 copy-done.6
  12.0 1.2 %convolution_convert_fusion.2 = bf16[16,1024]{1,0:T(8,128)(2,1)S(1)} fusion(bf16[256,1024]{1,0:T(8,128)(2,1)} %param.23, f32[2,8,2,128]{3,2,1,0:T(2,128)S(1)} %bitcast.43, f32[256]{0:T(256)S(1)} %bitcast.47), kind=kOutput, calls=%fused_computation.10 | convolution fusion | flops 8413184 | bytes 574464 | tf_op jit(solution)/shard_map/dot_general | solution.py:53
  13.2 10.0 %psum.7 = bf16[16,1024]{1,0:T(8,128)(2,1)S(1)} all-reduce(bf16[16,1024]{1,0:T(8,128)(2,1)S(1)} %convolution_convert_fusion.2), channel_id=1, replica_groups=mesh['ep'=16,'tp'=2] {'tp'}, use_global_device_ids=true, to_apply=%region_3.4 | all-reduce | flops 16384 | bytes 65536 | tf_op jit(solution)/shard_map/psum | solution.py:54
  23.2 0.0 copy-done.3
  23.2 0.1 fusion.17
  23.3 0.0 copy-done.5
  23.3 0.3 convolution_convert_fusion
  23.6 0.9 %reshape.168 = bf16[16,12,1024]{2,1,0:T(8,128)(2,1)} reshape(bf16[192,1024]{1,0:T(8,128)(2,1)S(1)} %convolution_convert_fusion) | data formatting | bytes 786432 | tf_op jit(solution)/shard_map/reshape | solution.py:89
  24.5 5.9 %all-to-all-start = ((bf16[16,12,1024]{2,1,0:T(8,128)(2,1)}), bf16[16,12,1024]{2,1,0:T(8,128)(2,1)S(1)}, u32[]{:S(2)}, u32[]{:S(2)}) async-start(bf16[16,12,1024]{2,1,0:T(8,128)(2,1)} %reshape.168), calls=%async_computation | async-start | bytes 1048576 | tf_op jit(solution)/shard_map/all_to_all | solution.py:91
  30.5 0.0 copy-done.9
  30.5 0.2 fusion.42
  30.7 0.1 copy.76
  30.8 0.0 copy-done.8
  30.8 0.2 convolution_exponential_fusion
  31.0 0.1 copy.74
  31.1 0.1 copy.75
  31.1 13.6 %all-to-all-done = bf16[16,12,1024]{2,1,0:T(8,128)(2,1)S(1)} async-done(((bf16[16,12,1024]{2,1,0:T(8,128)(2,1)}), bf16[16,12,1024]{2,1,0:T(8,128)(2,1)S(1)}, u32[]{:S(2)}, u32[]{:S(2)}) %all-to-all-start) | async-done | bytes 393248 | tf_op jit(solution)/shard_map/all_to_all | solution.py:91
  44.7 0.1 reshape.169
  44.8 0.0 copy-done
  44.8 0.4 fusion.11
  45.2 0.0 copy-done.7
  45.2 0.0 copy-start.2
  45.2 0.4 fusion.1
  45.6 0.0 copy-start.4
  45.6 7.6 %all-gather = bf16[192,1024]{1,0:T(8,128)(2,1)S(1)} all-gather(bf16[192,512]{1,0:T(8,128)(2,1)S(1)} %fusion.1), channel_id=2, replica_groups=mesh['ep'=16,'tp'=2] {'tp'}, dimensions={1}, use_global_device_ids=true | all-gather | bytes 589824 | tf_op jit(solution)/shard_map/all_gather | solution.py:99
  53.2 0.0 copy-done.2
  53.2 0.4 fusion.2
  53.6 0.3 copy.92
  53.9 0.5 broadcast.119
  54.4 1.8 %reduce.1 = bf16[192,512]{1,0:T(8,128)(2,1)S(1)} reduce(bf16[192,1,512]{2,1,0:T(2,128)(2,1)S(1)} %bitcast.41, bf16[]{:T(256)} %broadcast.119), dimensions={1}, to_apply=%bitcast.40.reduce_sub_computation | reduce | bytes 393218
  56.3 0.8 %reshape.179 = bf16[16,2,3072]{2,1,0:T(2,128)(2,1)} reshape(bf16[192,512]{1,0:T(8,128)(2,1)S(1)} %reduce.1) | data formatting | bytes 393216
  57.0 4.4 %all-to-all-start.1 = ((bf16[16,2,3072]{2,1,0:T(2,128)(2,1)}), bf16[16,2,3072]{2,1,0:T(2,128)(2,1)S(1)}, u32[]{:S(2)}, u32[]{:S(2)}) async-start(bf16[16,2,3072]{2,1,0:T(2,128)(2,1)} %reshape.179), calls=%async_computation.1 | async-start | bytes 393216 | tf_op jit(solution)/shard_map/all_to_all | solution.py:103
  61.5 0.0 copy-done.4
  61.5 0.2 select_reduce_fusion
  61.7 8.7 %all-to-all-done.1 = bf16[16,2,3072]{2,1,0:T(2,128)(2,1)S(1)} async-done(((bf16[16,2,3072]{2,1,0:T(2,128)(2,1)}), bf16[16,2,3072]{2,1,0:T(2,128)(2,1)S(1)}, u32[]{:S(2)}, u32[]{:S(2)}) %all-to-all-start.1) | async-done | bytes 196640 | tf_op jit(solution)/shard_map/all_to_all | solution.py:103
  70.4 0.1 reshape.180
  70.5 0.2 fusion.3
  70.8 0.6 add_convert_fusion
  (13 shorter events, 0.1 us)
Async XLA Ops:
  0.6 44.2 %copy-start = (bf16[1,1024,512]{2,1,0:T(8,128)(2,1)S(1)}, bf16[1,1024,512]{2,1,0:T(8,128)(2,1)}, u32[]{:S(2)}) copy-start(bf16[1,1024,512]{2,1,0:T(8,128)(2,1)} %param.29) | copy-start | bytes 3145732
  0.6 8.0 %copy-start.1 = (f32[16,2,128,128]{3,2,1,0:T(8,128)S(1)}, f32[16,2,128,128]{3,2,1,0:T(8,128)}, u32[]{:S(2)}) copy-start(f32[16,2,128,128]{3,2,1,0:T(8,128)} %param.17) | copy-start | bytes 6291460
  8.6 3.4 %copy-start.6 = (f32[2,128]{1,0:T(2,128)S(1)}, f32[2,128]{1,0:T(2,128)}, u32[]{:S(2)}) copy-start(f32[2,128]{1,0:T(2,128)} %param.22) | copy-start | bytes 3076
  8.6 14.5 %copy-start.3 = (bf16[16,1024]{1,0:T(8,128)(2,1)S(1)}, bf16[16,1024]{1,0:T(8,128)(2,1)}, u32[]{:S(2)}) copy-start(bf16[16,1024]{1,0:T(8,128)(2,1)} %param.16) | copy-start | bytes 98308
  8.7 14.7 %copy-start.5 = (f32[1024]{0:T(1024)S(1)}, f32[1024]{0:T(1024)}, u32[]{:S(2)}) copy-start(f32[1024]{0:T(1024)} %param.25) | copy-start | bytes 12292
  11.7 18.8 %copy-start.9 = (bf16[1024,4]{0,1:T(4,128)(2,1)S(1)}, bf16[1024,4]{0,1:T(4,128)(2,1)}, u32[]{:S(2)}) copy-start(bf16[1024,4]{0,1:T(4,128)(2,1)} %param.26) | copy-start | bytes 24580
  11.7 19.1 %copy-start.8 = (bf16[1024,16]{0,1:T(8,128)(2,1)S(1)}, bf16[1024,16]{0,1:T(8,128)(2,1)}, u32[]{:S(2)}) copy-start(bf16[1024,16]{0,1:T(8,128)(2,1)} %param.27) | copy-start | bytes 98308
  24.5 20.7 %copy-start.7 = (bf16[1,1024,512]{2,1,0:T(8,128)(2,1)S(1)}, bf16[1,1024,512]{2,1,0:T(8,128)(2,1)}, u32[]{:S(2)}) copy-start(bf16[1,1024,512]{2,1,0:T(8,128)(2,1)} %param.30) | copy-start | bytes 3145732
  24.5 20.2 %all-to-all-start = ((bf16[16,12,1024]{2,1,0:T(8,128)(2,1)}), bf16[16,12,1024]{2,1,0:T(8,128)(2,1)S(1)}, u32[]{:S(2)}, u32[]{:S(2)}) async-start(bf16[16,12,1024]{2,1,0:T(8,128)(2,1)} %reshape.168), calls=%async_computation | async-start | bytes 1048576 | tf_op jit(solution)/shard_map/all_to_all | solution.py:91
  45.2 8.0 %copy-start.2 = (bf16[1,1024,512]{2,1,0:T(8,128)(2,1)S(1)}, bf16[1,1024,512]{2,1,0:T(8,128)(2,1)}, u32[]{:S(2)}) copy-start(bf16[1,1024,512]{2,1,0:T(8,128)(2,1)} %param.31) | copy-start | bytes 3145732
  45.6 15.8 %copy-start.4 = (s32[16,6]{0,1:T(8,128)S(1)}, s32[16,6]{0,1:T(8,128)}, u32[]{:S(2)}) copy-start(s32[16,6]{0,1:T(8,128)} %param.28) | copy-start | bytes 1156
  57.0 13.4 %all-to-all-start.1 = ((bf16[16,2,3072]{2,1,0:T(2,128)(2,1)}), bf16[16,2,3072]{2,1,0:T(2,128)(2,1)S(1)}, u32[]{:S(2)}, u32[]{:S(2)}) async-start(bf16[16,2,3072]{2,1,0:T(2,128)(2,1)} %reshape.179), calls=%async_computation.1 | async-start | bytes 393216 | tf_op jit(solution)/shard_map/all_to_all | solution.py:103
where the time goes:
time: 71.9 us; the launch traced here: 71.4 us
  waiting for transfers between devices  22.3 us (31%)
  blocking collectives  17.6 us (24%)
  starting transfers between devices  10.3 us (14%)
  other arithmetic  8.77 us (12%)
  matrix products  7.21 us (10%)
  local copies, waits for them, and re-layouts  4.28 us (6%)
  between operations  0.95 us (1%)
    all_to_all x1, waiting for transfers between devices, local(): lax.all_to_all(outgoing, 'ep', split_axis=0, concat_axis=1, tiled=True)  13.6 us
    psum x1, blocking collectives, local(): mixed = lax.psum(head_part.astype(jnp.bfloat16), 'tp')  9.95 us
    all_to_all x1, waiting for transfers between devices, local(): lax.all_to_all(produced, 'ep', split_axis=1, concat_axis=0, tiled=True)  8.72 us
    all_gather x1, blocking collectives, local(): lax.all_gather(hidden, 'tp', axis=2, tiled=True)  7.6 us
    all_to_all x1, starting transfers between devices, local(): lax.all_to_all(outgoing, 'ep', split_axis=0, concat_axis=1, tiled=True)  5.92 us
    all_to_all x1, starting transfers between devices, local(): lax.all_to_all(produced, 'ep', split_axis=1, concat_axis=0, tiled=True)  4.41 us
    reduce_sum x1, other arithmetic, local(): readout = jnp.sum(new_state * query[..., None], axis=2)  3.02 us
    unnamed x24, local copies, waits for them, and re-layouts  2.4 us
  transfers between devices with their start and end apart: 2, of which 2 were waited for; matrix products, arithmetic and copies ran while one was open for 1% of the time, Pallas kernels for 0%

commit v1 on v0

--- a/solution.py
+++ b/solution.py
@@ -88,7 +88,10 @@
         .astype(jnp.bfloat16)
         .reshape(experts, capacity, model_width)
     )
-    arrived = lax.all_to_all(outgoing, "ep", split_axis=0, concat_axis=1, tiled=True)
+    arrived = jnp.concatenate(
+        lax.all_to_all(jnp.stack(jnp.split(outgoing, lax.axis_size("ep"), axis=0)), "ep", 0, 0),
+        axis=1,
+    )
     gate_hidden = jnp.einsum(
         "erd,edf->erf", arrived, gate_weight, preferred_element_type=jnp.float32
     )

time: 71.9 us -> 80.7 us (1.12)
  local copies, waits for them, and re-layouts: 4.28 us -> 13.1 us
    unnamed x24 -> x39, local copies, waits for them, and re-layouts: 2.4 us -> 11.5 us
    reshape x1 -> x0, local copies, waits for them, and re-layouts: 0.88 us -> none  [local(): outgoing = jnp.dot(spread, ffn_in, preferred_element_type=jnp.float32).as...]
where the time goes in v1:
time: 80.7 us; the launch traced here: 80.1 us
  waiting for transfers between devices  22.3 us (28%)
  blocking collectives  17.6 us (22%)
  local copies, waits for them, and re-layouts  13.1 us (16%)
  starting transfers between devices  10.2 us (13%)
  other arithmetic  8.77 us (11%)
  matrix products  7.2 us (9%)
  between operations  0.96 us (1%)
    all_to_all x1, waiting for transfers between devices, local(): lax.all_to_all(jnp.stack(jnp.split(outgoing, lax.axis_size('ep'), axis=0)...  13.6 us
    unnamed x39, local copies, waits for them, and re-layouts  11.5 us
    psum x1, blocking collectives, local(): mixed = lax.psum(head_part.astype(jnp.bfloat16), 'tp')  9.95 us
    all_to_all x1, waiting for transfers between devices, local(): lax.all_to_all(produced, 'ep', split_axis=1, concat_axis=0, tiled=True)  8.72 us
    all_gather x1, blocking collectives, local(): lax.all_gather(hidden, 'tp', axis=2, tiled=True)  7.62 us
    all_to_all x1, starting transfers between devices, local(): lax.all_to_all(jnp.stack(jnp.split(outgoing, lax.axis_size('ep'), axis=0)...  5.79 us
    all_to_all x1, starting transfers between devices, local(): lax.all_to_all(produced, 'ep', split_axis=1, concat_axis=0, tiled=True)  4.41 us
    reduce_sum x1, other arithmetic, local(): readout = jnp.sum(new_state * query[..., None], axis=2)  3.02 us
  transfers between devices with their start and end apart: 2, of which 2 were waited for; matrix products, arithmetic and copies ran while one was open for 1% of the time, Pallas kernels for 0%

profile of v1, /device:TPU:0, one launch (start us, length us, event | category | flops | bytes accessed | tf_op | source)
XLA Modules:
  0.0 80.1 jit_solution(11627043963104435541)
XLA Ops:
  0.6 0.0 copy-start
  0.7 0.9 %copy.77 = s32[16,6]{1,0:T(8,128)S(1)} copy(s32[16,6]{0,1:T(8,128)} %param.28) | data formatting | bytes 768 | tf_op args[12]
  1.6 0.1 eq.73
  1.7 0.1 fusion.25
  1.8 0.1 reduce_window_sum.11
  1.9 0.2 select_reduce_fusion.2
  2.1 0.1 reduce_sum.110
  2.1 0.1 copy.78
  2.2 0.7 multiply_add_fusion.1
  2.9 0.1 convert_reduce_fusion
  3.0 0.9 %fusion.20 = f32[16]{0:T(128)S(1)} fusion(bf16[16,1024]{1,0:T(8,128)(2,1)} %param.16), kind=kLoop, calls=%fused_computation.37 | loop fusion | flops 49136 | bytes 32832 | tf_op jit(solution)/shard_map/reduce_sum | solution.py:10
  3.9 1.3 %divide_multiply_fusion = f32[16,256]{1,0:T(8,128)S(1)} fusion(bf16[1024,256]{1,0:T(8,128)(2,1)} %param.18, bf16[16,1024]{1,0:T(8,128)(2,1)} %param.16, f32[1024]{0:T(1024)} %param.24, f32[16]{0:T(128)S(1)} %add_rsqrt_fusion.2), kind=kOutput, calls=%fused_computation.85 | convolution fusion | flops 8470528 | bytes 577600 | tf_op jit(solution)/shard_map/dot_general | solution.py:38
  5.3 1.3 %fusion.33 = f32[16,256]{1,0:T(8,128)S(1)} fusion(bf16[1024,256]{1,0:T(8,128)(2,1)} %param.20, bf16[16,1024]{1,0:T(8,128)(2,1)} %param.16, f32[1024]{0:T(1024)} %param.24, f32[16]{0:T(128)S(1)} %add_rsqrt_fusion.2), kind=kOutput, calls=%fused_computation.99 | convolution fusion | flops 8454144 | bytes 577600 | tf_op jit(solution)/shard_map/dot_general | solution.py:40
  6.6 0.7 broadcast_subtract_fusion.1
  7.3 1.3 %fusion.8 = f32[16,256]{1,0:T(8,128)S(1)} fusion(bf16[1024,256]{1,0:T(8,128)(2,1)} %param.19, f32[256]{0:T(256)S(1)} %broadcast_subtract_fusion.1, f32[256]{0:T(256)} %param.21, bf16[16,1024]{1,0:T(8,128)(2,1)} %param.16, f32[1024]{0:T(1024)} %param.24, f32[16]{0:T(128)S(1)} %add_rsqrt_fusion.2), kind=kOutput, calls=%fused_computation.16 | convolution fusion | flops 8474624 | bytes 579648 | tf_op jit(solution)/shard_map/dot_general | solution.py:39
  8.6 0.0 copy-start.3
  8.7 0.0 copy-start.5
  8.7 3.0 %multiply_reduce_fusion = (f32[16,2,128]{2,1,0:T(2,128)S(1)}, f32[16,2,128,128]{3,2,1,0:T(8,128)}) fusion(f32[16,2,128]{2,1,0:T(2,128)S(1)} %mul.173, f32[16,2,128]{2,1,0:T(2,128)S(1)} %mul.169, f32[16,2,128]{2,1,0:T(2,128)S(1)} %broadcast_subtract_fusion, f32[16,2,128,128]{3,2,1,0:T(8,128)S(1)} %copy-done.1, f32[16,2,128]{2,1,0:T(2,128)S(1)} %mul.165), kind=kLoop, calls=%fused_computation.1 | loop fusion | flops 2617344 | bytes 4276224 | tf_op jit(solution)/shard_map/reduce_sum | solution.py:47
  11.7 0.1 fusion.27
  11.8 0.1 copy.73
  11.9 0.1 broadcast_multiply_fusion
  12.0 1.2 %convolution_convert_fusion.2 = bf16[16,1024]{1,0:T(8,128)(2,1)S(1)} fusion(bf16[256,1024]{1,0:T(8,128)(2,1)} %param.23, f32[2,8,2,128]{3,2,1,0:T(2,128)S(1)} %bitcast.107, f32[256]{0:T(256)S(1)} %bitcast.111), kind=kOutput, calls=%fused_computation.10 | convolution fusion | flops 8413184 | bytes 574464 | tf_op jit(solution)/shard_map/dot_general | solution.py:53
  13.2 10.0 %psum.7 = bf16[16,1024]{1,0:T(8,128)(2,1)S(1)} all-reduce(bf16[16,1024]{1,0:T(8,128)(2,1)S(1)} %convolution_convert_fusion.2), channel_id=1, replica_groups=mesh['ep'=16,'tp'=2] {'tp'}, use_global_device_ids=true, to_apply=%region_3.4 | all-reduce | flops 16384 | bytes 65536 | tf_op jit(solution)/shard_map/psum | solution.py:54
  23.2 0.1 fusion.17
  23.3 0.3 convolution_convert_fusion
  23.6 0.6 constant_dynamic-update-slice_fusion.15
  24.2 0.6 constant_dynamic-update-slice_fusion.14
  24.9 0.6 constant_dynamic-update-slice_fusion.13
  25.5 0.6 constant_dynamic-update-slice_fusion.12
  26.1 0.6 constant_dynamic-update-slice_fusion.11
  26.7 0.6 constant_dynamic-update-slice_fusion.10
  27.3 0.6 constant_dynamic-update-slice_fusion.9
  27.9 0.6 constant_dynamic-update-slice_fusion.8
  28.5 0.6 constant_dynamic-update-slice_fusion.7
  29.1 0.6 constant_dynamic-update-slice_fusion.6
  29.7 0.6 constant_dynamic-update-slice_fusion.5
  30.3 0.6 constant_dynamic-update-slice_fusion.4
  31.0 0.6 constant_dynamic-update-slice_fusion.3
  31.6 0.6 constant_dynamic-update-slice_fusion.2
  32.2 0.6 constant_dynamic-update-slice_fusion.1
  32.8 0.6 constant_dynamic-update-slice_fusion
  33.4 5.8 %all-to-all-start = ((bf16[16,1,12,1024]{3,2,1,0:T(8,128)(2,1)}), bf16[16,1,12,1024]{3,2,1,0:T(8,128)(2,1)S(1)}, u32[]{:S(2)}, u32[]{:S(2)}) async-start(bf16[16,1,12,1024]{3,2,1,0:T(8,128)(2,1)} %constant_dynamic-update-slice_fusion), calls=%async_computation | async-start | bytes 1048576 | tf_op jit(solution)/shard_map/all_to_all | solution.py:92
  39.2 0.2 fusion.42
  39.4 0.1 copy.76
  39.5 0.2 convolution_exponential_fusion
  39.7 0.1 copy.74
  39.8 0.1 copy.75
  39.9 13.6 %all-to-all-done = bf16[16,1,12,1024]{3,2,1,0:T(8,128)(2,1)S(1)} async-done(((bf16[16,1,12,1024]{3,2,1,0:T(8,128)(2,1)}), bf16[16,1,12,1024]{3,2,1,0:T(8,128)(2,1)S(1)}, u32[]{:S(2)}, u32[]{:S(2)}) %all-to-all-start) | async-done | bytes 393248 | tf_op jit(solution)/shard_map/all_to_all | solution.py:92
  53.5 0.1 reshape.196
  53.6 0.4 fusion.11
  54.0 0.4 fusion.1
  54.4 0.0 copy-start.4
  54.4 7.6 %all-gather = bf16[192,1024]{1,0:T(8,128)(2,1)S(1)} all-gather(bf16[192,512]{1,0:T(8,128)(2,1)S(1)} %fusion.1), channel_id=2, replica_groups=mesh['ep'=16,'tp'=2] {'tp'}, dimensions={1}, use_global_device_ids=true | all-gather | bytes 589824 | tf_op jit(solution)/shard_map/all_gather | solution.py:102
  62.0 0.4 fusion.2
  62.4 0.3 copy.92
  62.7 0.5 broadcast.119
  63.2 1.8 %reduce.1 = bf16[192,512]{1,0:T(8,128)(2,1)S(1)} reduce(bf16[192,1,512]{2,1,0:T(2,128)(2,1)S(1)} %bitcast.105, bf16[]{:T(256)} %broadcast.119), dimensions={1}, to_apply=%bitcast.104.reduce_sub_computation | reduce | bytes 393218
  65.0 0.8 reshape.206
  65.8 4.4 %all-to-all-start.1 = ((bf16[16,2,3072]{2,1,0:T(2,128)(2,1)}), bf16[16,2,3072]{2,1,0:T(2,128)(2,1)S(1)}, u32[]{:S(2)}, u32[]{:S(2)}) async-start(bf16[16,2,3072]{2,1,0:T(2,128)(2,1)} %reshape.206), calls=%async_computation.1 | async-start | bytes 393216 | tf_op jit(solution)/shard_map/all_to_all | solution.py:106
  70.2 0.2 select_reduce_fusion
  70.4 8.7 %all-to-all-done.1 = bf16[16,2,3072]{2,1,0:T(2,128)(2,1)S(1)} async-done(((bf16[16,2,3072]{2,1,0:T(2,128)(2,1)}), bf16[16,2,3072]{2,1,0:T(2,128)(2,1)S(1)}, u32[]{:S(2)}, u32[]{:S(2)}) %all-to-all-start.1) | async-done | bytes 196640 | tf_op jit(solution)/shard_map/all_to_all | solution.py:106
  79.2 0.1 reshape.207
  79.3 0.2 fusion.3
  79.5 0.6 add_convert_fusion
  (28 shorter events, 0.2 us)
Async XLA Ops:
  0.6 52.9 %copy-start = (bf16[1,1024,512]{2,1,0:T(8,128)(2,1)S(1)}, bf16[1,1024,512]{2,1,0:T(8,128)(2,1)}, u32[]{:S(2)}) copy-start(bf16[1,1024,512]{2,1,0:T(8,128)(2,1)} %param.29) | copy-start | bytes 3145732
  0.6 8.0 %copy-start.1 = (f32[16,2,128,128]{3,2,1,0:T(8,128)S(1)}, f32[16,2,128,128]{3,2,1,0:T(8,128)}, u32[]{:S(2)}) copy-start(f32[16,2,128,128]{3,2,1,0:T(8,128)} %param.17) | copy-start | bytes 6291460
  8.6 3.4 %copy-start.6 = (f32[2,128]{1,0:T(2,128)S(1)}, f32[2,128]{1,0:T(2,128)}, u32[]{:S(2)}) copy-start(f32[2,128]{1,0:T(2,128)} %param.22) | copy-start | bytes 3076
  8.6 14.5 %copy-start.3 = (bf16[16,1024]{1,0:T(8,128)(2,1)S(1)}, bf16[16,1024]{1,0:T(8,128)(2,1)}, u32[]{:S(2)}) copy-start(bf16[16,1024]{1,0:T(8,128)(2,1)} %param.16) | copy-start | bytes 98308
  8.7 14.7 %copy-start.5 = (f32[1024]{0:T(1024)S(1)}, f32[1024]{0:T(1024)}, u32[]{:S(2)}) copy-start(f32[1024]{0:T(1024)} %param.25) | copy-start | bytes 12292
  11.7 27.5 %copy-start.9 = (bf16[1024,4]{0,1:T(4,128)(2,1)S(1)}, bf16[1024,4]{0,1:T(4,128)(2,1)}, u32[]{:S(2)}) copy-start(bf16[1024,4]{0,1:T(4,128)(2,1)} %param.26) | copy-start | bytes 24580
  11.7 27.8 %copy-start.8 = (bf16[1024,16]{0,1:T(8,128)(2,1)S(1)}, bf16[1024,16]{0,1:T(8,128)(2,1)}, u32[]{:S(2)}) copy-start(bf16[1024,16]{0,1:T(8,128)(2,1)} %param.27) | copy-start | bytes 98308
  32.2 21.8 %copy-start.7 = (bf16[1,1024,512]{2,1,0:T(8,128)(2,1)S(1)}, bf16[1,1024,512]{2,1,0:T(8,128)(2,1)}, u32[]{:S(2)}) copy-start(bf16[1,1024,512]{2,1,0:T(8,128)(2,1)} %param.30) | copy-start | bytes 3145732
  33.4 20.1 %all-to-all-start = ((bf16[16,1,12,1024]{3,2,1,0:T(8,128)(2,1)}), bf16[16,1,12,1024]{3,2,1,0:T(8,128)(2,1)S(1)}, u32[]{:S(2)}, u32[]{:S(2)}) async-start(bf16[16,1,12,1024]{3,2,1,0:T(8,128)(2,1)} %constant_dynamic-update-slice_fusion), calls=%async_computation | async-start | bytes 1048576 | tf_op jit(solution)/shard_map/all_to_all | solution.py:92
  54.0 8.0 %copy-start.2 = (bf16[1,1024,512]{2,1,0:T(8,128)(2,1)S(1)}, bf16[1,1024,512]{2,1,0:T(8,128)(2,1)}, u32[]{:S(2)}) copy-start(bf16[1,1024,512]{2,1,0:T(8,128)(2,1)} %param.31) | copy-start | bytes 3145732
  54.4 15.9 %copy-start.4 = (s32[16,6]{0,1:T(8,128)S(1)}, s32[16,6]{0,1:T(8,128)}, u32[]{:S(2)}) copy-start(s32[16,6]{0,1:T(8,128)} %param.28) | copy-start | bytes 1156
  65.8 13.4 %all-to-all-start.1 = ((bf16[16,2,3072]{2,1,0:T(2,128)(2,1)}), bf16[16,2,3072]{2,1,0:T(2,128)(2,1)S(1)}, u32[]{:S(2)}, u32[]{:S(2)}) async-start(bf16[16,2,3072]{2,1,0:T(2,128)(2,1)} %reshape.206), calls=%async_computation.1 | async-start | bytes 393216 | tf_op jit(solution)/shard_map/all_to_all | solution.py:106
